TPU v7x, 512 devices: a whole 4x8x8 slice. The times are simulated.
512 devices in a mesh: sp: 32 (over z, x), tp: 16 (over y, core).
Axes of the slice: x: 4, y: 8, z: 8, core: 2. Of those that a mesh axis runs over, the one named last changes fastest.
Arguments:
- in_gate: bfloat16 [1024, 8192], P('tp', 'sp'), may hold values from -6 to 6
- out_gate: bfloat16 [1024, 8192], P('tp', 'sp'), may hold values from -6 to 6
- values: bfloat16 [1024, 8192], P('tp', 'sp'), may hold values from -6 to 6
- conv_taps: bfloat16 [3, 1024], P(None, 'tp'), may hold values from -3.5 to 3.5
- doc_ids: int32 [8192], P('sp'), may hold values from 0 to 7, as said below
- residual: bfloat16 [8192, 2048], P('sp'), may hold values from -6 to 6
- out_weight: bfloat16 [1024, 2048], P('tp'), may hold values from -0.1875 to 0.1875
- norm_gain: bfloat16 [2048], replicated, may hold values from 0.099609375 to 1.8984375
- routes: int32 [8192, 2], P('sp'), may hold values from 0 to 31, all different within a row; in each aligned block of 256 rows (0 to 255, 256 to 511, ...) at most 24 rows name the same one
- route_weights: float32 [8192, 2], P('sp'), may hold values from 0.2 to 1
- expert_gate: bfloat16 [32, 2048, 4224], P('sp', None, 'tp'), may hold values from -0.125 to 0.125
- expert_up: bfloat16 [32, 2048, 4224], P('sp', None, 'tp'), may hold values from -0.125 to 0.125
- expert_down: bfloat16 [32, 4224, 2048], P('sp', 'tp'), may hold values from -0.09375 to 0.09375
Outputs:
- merged: bfloat16 [8192, 2048], P('sp', 'tp')
Inputs may be any that keep to these rules, and one draw needn't show every extreme that they name: `routes`: each row names 2 different experts. Within the rows of one index of sp (aligned blocks of 256 rows) no expert is named more than 24 times, a bound that some expert reaches in some blocks. `doc_ids`: never falls along the sequence; starts at 0 and rises by one at each of 7 document starts, each number used.
All inputs are finite; a program needn't handle non-finite values.
Results may differ from a plain program's by a relative error of at most 0.019.
Values may be sent and summed in bfloat16 or wider, within the bound.
A program may use at most 64 MiB of HBM per device.

v0:
```python
import jax
import jax.numpy as jnp
from jax import lax
from jax.sharding import PartitionSpec as P

EPSILON = 1e-06


def shifted(x, axis, by):
    count = lax.axis_size(axis)
    pairs = [(i, i + by) for i in range(count) if 0 <= i + by < count]
    return lax.ppermute(x, axis, pairs)


def in_blocks(x, dim, count):
    before, after = (x.shape[:dim], x.shape[dim + 1 :])
    return jnp.moveaxis(x.reshape(*before, count, -1, *after), dim, 0)


def sum_at_owner(x, axis, dim):
    count = lax.axis_size(axis)
    parts = lax.all_to_all(in_blocks(x, dim, count), axis, 0, 0, tiled=True)
    return jnp.sum(parts.astype(jnp.float32), axis=0)


def copy_for_each(x, axis):
    copies = jnp.broadcast_to(x, (lax.axis_size(axis), *x.shape))
    return lax.all_to_all(copies, axis, split_axis=0, concat_axis=0, tiled=True)


def taken_together(x, axis):
    everything = copy_for_each(x, axis)
    return jnp.sum(everything, axis=0)


def shards(
    in_gate,
    out_gate,
    values,
    conv_taps,
    doc_ids,
    residual,
    out_weight,
    norm_gain,
    routes,
    route_weights,
    expert_gate,
    expert_up,
    expert_down,
):
    gated_in = (in_gate.astype(jnp.float32) * values.astype(jnp.float32)).astype(jnp.bfloat16)
    tail_rows, tail_docs = shifted((gated_in[:, -2:], doc_ids[-2:]), "sp", 1)
    extended = lax.optimization_barrier(jnp.concatenate([tail_rows, gated_in], axis=1)).astype(
        jnp.float32
    )
    docs_ext = jnp.concatenate([tail_docs, doc_ids])
    length = doc_ids.shape[0]
    near_mask = (docs_ext[1 : length + 1] == doc_ids).astype(jnp.float32)
    far_mask = (docs_ext[0:length] == doc_ids).astype(jnp.float32)
    tap_values = conv_taps.astype(jnp.float32)
    convolved = (
        tap_values[2][:, None] * extended[:, 2:]
        + tap_values[1][:, None] * extended[:, 1 : length + 1] * near_mask[None, :]
        + tap_values[0][:, None] * extended[:, 0:length] * far_mask[None, :]
    )
    mixed_rows = (out_gate.astype(jnp.float32) * convolved).astype(jnp.bfloat16)
    partial_value = lax.dot_general(
        mixed_rows, out_weight, (((0,), (0,)), ((), ())), preferred_element_type=jnp.float32
    )
    tp_count = lax.axis_size("tp")
    model_width = residual.shape[1]
    share_width = model_width // tp_count
    column = lax.axis_index("tp") * share_width
    share_sum = sum_at_owner(partial_value.astype(jnp.bfloat16), "tp", 1)
    stream_cols = (
        lax.dynamic_slice_in_dim(residual, column, share_width, 1).astype(jnp.float32) + share_sum
    )
    square_total = taken_together(jnp.sum(stream_cols * stream_cols, axis=1, keepdims=True), "tp")
    inv_rms = lax.rsqrt(square_total / model_width + EPSILON)
    gain_cols = lax.dynamic_slice_in_dim(norm_gain, column, share_width, 0).astype(jnp.float32)
    own_cols = (stream_cols * inv_rms * gain_cols[None, :]).astype(jnp.bfloat16)
    tokens = routes.shape[0]
    top_count = routes.shape[1]
    experts = lax.axis_size("sp")
    capacity = 3 * tokens * top_count // (2 * experts)
    chosen = routes.reshape(-1)
    hits_table = (chosen[:, None] == jnp.arange(experts, dtype=jnp.int32)[None, :]).astype(
        jnp.int32
    )
    earlier = jnp.cumsum(hits_table, axis=0) - hits_table
    ranked = jnp.sum(earlier * hits_table, axis=1)
    slot_index = chosen * capacity + ranked
    owners = jnp.arange(tokens * top_count, dtype=jnp.int32) // top_count
    source = jnp.zeros((experts * capacity,), jnp.int32).at[slot_index].set(owners)
    filled = jnp.zeros((experts * capacity,), jnp.bool_).at[slot_index].set(True)
    gate_weight = expert_gate[0]
    up_weight = expert_up[0]
    down_weight = expert_down[0]
    picked = jnp.where(
        filled[:, None], jnp.take(own_cols, source, axis=0), jnp.zeros((), jnp.bfloat16)
    ).reshape(experts, capacity, share_width)
    arrived = lax.all_to_all(picked, "sp", split_axis=0, concat_axis=0, tiled=True)
    slot_count = arrived.shape[1]
    row_block = arrived.reshape(-1, share_width)
    piece_cols = lax.all_gather(row_block, "tp", axis=1, tiled=True)
    gate_sum = jnp.dot(piece_cols, gate_weight, preferred_element_type=jnp.float32)
    up_sum = jnp.dot(piece_cols, up_weight, preferred_element_type=jnp.float32)
    hidden = (jax.nn.silu(gate_sum) * up_sum).astype(jnp.bfloat16)
    down_sum = jnp.dot(hidden, down_weight, preferred_element_type=jnp.float32)
    summed = lax.psum_scatter(down_sum.astype(jnp.bfloat16), "tp", scatter_dimension=1, tiled=True)
    returned = lax.all_to_all(
        summed.reshape(experts, slot_count, share_width),
        "sp",
        split_axis=0,
        concat_axis=0,
        tiled=True,
    )
    results = jnp.take(returned.reshape(experts * capacity, share_width), slot_index, axis=0)
    results = results.astype(jnp.float32).reshape(tokens, top_count, share_width)
    blended = jnp.sum(route_weights[:, :, None] * results, axis=1)
    return (stream_cols + blended).astype(jnp.bfloat16)


def solution(mesh):
    placed = (
        P("tp", "sp"),
        P("tp", "sp"),
        P("tp", "sp"),
        P(None, "tp"),
        P("sp"),
        P("sp", None),
        P("tp", None),
        P(),
        P("sp", None),
        P("sp", None),
        P("sp", None, "tp"),
        P("sp", None, "tp"),
        P("sp", "tp", None),
    )
    return jax.shard_map(
        shards, mesh=mesh, in_specs=placed, out_specs=P("sp", "tp"), check_vma=False
    )
```

profile of v0, /device:TPU:25, one launch (start us, length us, event | category | flops | bytes accessed | tf_op | source)
XLA Modules:
  0.0 249.2 jit_solution(15345662534989394620)
XLA Ops:
  6.5 0.9 multiply_convert_fusion.1
  7.5 3.1 %collective-permute-start = (bf16[64,2]{1,0:T(8,128)(2,1)S(1)}, bf16[64,2]{1,0:T(8,128)(2,1)S(1)}, u32[]{:S(2)}, u32[]{:S(2)}) collective-permute-start(bf16[64,2]{1,0:T(8,128)(2,1)S(1)} %slice.52), channel_id=1, source_target_pairs={{0,16},{16,32},{32,48},{48,64},{64,80},{80,96},{96,112},{112,128},... | collective-permute-start | bytes 776 | tf_op jit(solution)/shard_map/ppermute | solution.py:12
  10.6 0.8 slice.41
  11.4 3.1 %collective-permute-start.1 = (s32[2]{0:T(128)S(1)}, s32[2]{0:T(128)S(1)}, u32[]{:S(2)}, u32[]{:S(2)}) collective-permute-start(s32[2]{0:T(128)S(1)} %slice.41), channel_id=1, source_target_pairs={{0,16},{16,32},{32,48},{48,64},{64,80},{80,96},{96,112},{112,128},... | collective-permute-start | bytes 32 | tf_op jit(solution)/shard_map/ppermute | solution.py:12
  14.5 0.7 convert_element_type.64
  15.2 0.8 pad_add_fusion
  15.9 0.8 compare_convert_fusion.1
  16.8 1.5 fusion
  18.3 1.3 copy.41
  19.6 8.7 %all-to-all-start = ((bf16[16,256,128]{2,1,0:T(8,128)(2,1)}), bf16[16,256,128]{2,1,0:T(8,128)(2,1)S(1)}, u32[]{:S(2)}, u32[]{:S(2)}) async-start(bf16[16,256,128]{2,1,0:T(8,128)(2,1)} %bitcast.55), calls=%async_computation | async-start | bytes 2097152 | tf_op jit(solution)/shard_map/all_to_all | solution.py:22
  28.8 1.2 reduce-window.6
  30.7 2.4 scatter_custom_fusion.1
  33.2 21.4 %all-to-all-done = bf16[16,256,128]{2,1,0:T(8,128)(2,1)S(1)} async-done(((bf16[16,256,128]{2,1,0:T(8,128)(2,1)}), bf16[16,256,128]{2,1,0:T(8,128)(2,1)S(1)}, u32[]{:S(2)}, u32[]{:S(2)}) %all-to-all-start) | async-done | bytes 1048608 | tf_op jit(solution)/shard_map/all_to_all | solution.py:22
  54.7 1.0 multiply_reduce_fusion.1
  56.3 5.2 %all-to-all-start.1 = ((f32[16,256,1]{1,2,0:T(1,128)}), f32[16,256,1]{1,2,0:T(1,128)S(1)}, u32[]{:S(2)}, u32[]{:S(2)}) async-start(f32[16,256,1]{1,2,0:T(1,128)} %broadcast_in_dim.67), calls=%async_computation.1 | async-start | bytes 32768 | tf_op jit(solution)/shard_map/all_to_all | solution.py:28
  61.5 0.8 dynamic-slice_convert_fusion
  62.4 2.4 scatter_custom_fusion
  65.0 1.1 all-to-all-done.1
  66.1 0.9 multiply_convert_fusion
  67.0 1.9 gather_fusion
  69.2 25.0 %all_to_all.20 = bf16[32,24,128]{2,1,0:T(8,128)(2,1)} all-to-all(bf16[32,24,128]{2,1,0:T(8,128)(2,1)S(1)} %select_select_fusion), channel_id=1, replica_groups=mesh['sp'=32,'tp'=16] {'sp'}, dimensions={0} | all-to-all | bytes 393216 | tf_op jit(solution)/shard_map/all_to_all | solution.py:102
  94.3 41.9 %all-gather.2.cloned.1.call-done = bf16[768,2048]{1,0:T(8,128)(2,1)} async-done(((bf16[768,128]{1,0:T(8,128)(2,1)}), bf16[768,2048]{1,0:T(8,128)(2,1)}) %all-gather.2.cloned.1.call-update) | async-done | bytes 3145744 | tf_op jit(solution)/shard_map/all_gather | solution.py:105
  136.2 3.8 %fusion.4 = f32[768,264]{0,1:T(8,128)} fusion(bf16[768,2048]{1,0:T(8,128)(2,1)} %all-gather.2.cloned.1.call-done, bf16[1,2048,264]{1,2,0:T(8,128)(2,1)S(1)} %copy-done.3), kind=kOutput, calls=%fused_computation.12 | convolution fusion | flops 830472192 | bytes 5038080 | tf_op jit(solution)/shard_map/dot_general | solution.py:106
  140.0 7.3 %convolution_convert_fusion = bf16[768,2048]{1,0:T(8,128)(2,1)} fusion(bf16[1,264,2048]{2,1,0:T(8,128)(2,1)S(1)} %copy-done, bf16[768,2048]{1,0:T(8,128)(2,1)} %all-gather.2.cloned.1.call-done, bf16[1,2048,264]{1,2,0:T(8,128)(2,1)S(1)} %copy-done.4, f32[768,264]{0,1:T(8,128)} %fusion.4), kind=kOutput, calls=%fused_computation.4 | convolution fusion | flops 1663733760 | bytes 9265152 | tf_op jit(solution)/shard_map/dot_general | solution.py:109
  147.3 4.6 %copy.35 = bf16[768,2048]{0,1:T(8,128)(2,1)} copy(bf16[768,2048]{1,0:T(8,128)(2,1)} %convolution_convert_fusion) | data formatting | bytes 6291456
  152.0 64.2 %reduce-scatter.4.cloned.1.call-done = bf16[128,768]{1,0:T(8,128)(2,1)} async-done(((bf16[2048,768]{1,0:T(8,128)(2,1)}), bf16[128,768]{1,0:T(8,128)(2,1)}) %reduce-scatter.4.cloned.1.call-update) | async-done | bytes 196624
  216.1 1.7 copy.36
  217.9 10.1 %all-to-all-start.3 = ((bf16[32,24,128]{2,1,0:T(8,128)(2,1)}), bf16[32,24,128]{2,1,0:T(8,128)(2,1)S(1)}, u32[]{:S(2)}, u32[]{:S(2)}) async-start(bf16[32,24,128]{2,1,0:T(8,128)(2,1)} %bitcast.12), calls=%async_computation.3 | async-start | bytes 393216 | tf_op jit(solution)/shard_map/all_to_all | solution.py:111
  228.6 9.5 %all-to-all-done.3 = bf16[32,24,128]{2,1,0:T(8,128)(2,1)S(1)} async-done(((bf16[32,24,128]{2,1,0:T(8,128)(2,1)}), bf16[32,24,128]{2,1,0:T(8,128)(2,1)S(1)}, u32[]{:S(2)}, u32[]{:S(2)}) %all-to-all-start.3) | async-done | bytes 196640 | tf_op jit(solution)/shard_map/all_to_all | solution.py:111
  238.1 1.3 gather_fusion.1
  239.4 1.5 multiply_reduce_fusion
  240.9 1.5 add_convert_fusion
  (50 shorter events, 3.2 us)
Async XLA Ops:
  6.5 133.5 %copy-start = (bf16[1,264,2048]{2,1,0:T(8,128)(2,1)S(1)}, bf16[1,264,2048]{2,1,0:T(8,128)(2,1)}, u32[]{:S(2)}) copy-start(bf16[1,264,2048]{2,1,0:T(8,128)(2,1)} %param.25) | copy-start | bytes 3244036
  7.5 9.2 %collective-permute-start = (bf16[64,2]{1,0:T(8,128)(2,1)S(1)}, bf16[64,2]{1,0:T(8,128)(2,1)S(1)}, u32[]{:S(2)}, u32[]{:S(2)}) collective-permute-start(bf16[64,2]{1,0:T(8,128)(2,1)S(1)} %slice.52), channel_id=1, source_target_pairs={{0,16},{16,32},{32,48},{48,64},{64,80},{80,96},{96,112},{112,128},... | collective-permute-start | bytes 776 | tf_op jit(solution)/shard_map/ppermute | solution.py:12
  11.4 3.8 %collective-permute-start.1 = (s32[2]{0:T(128)S(1)}, s32[2]{0:T(128)S(1)}, u32[]{:S(2)}, u32[]{:S(2)}) collective-permute-start(s32[2]{0:T(128)S(1)} %slice.41), channel_id=1, source_target_pairs={{0,16},{16,32},{32,48},{48,64},{64,80},{80,96},{96,112},{112,128},... | collective-permute-start | bytes 32 | tf_op jit(solution)/shard_map/ppermute | solution.py:12
  18.3 10.0 %copy-start.1 = (s32[256,2]{0,1:T(2,128)S(1)}, s32[256,2]{0,1:T(2,128)}, u32[]{:S(2)}) copy-start(s32[256,2]{0,1:T(2,128)} %param.21) | copy-start | bytes 6148
  19.6 35.0 %all-to-all-start = ((bf16[16,256,128]{2,1,0:T(8,128)(2,1)}), bf16[16,256,128]{2,1,0:T(8,128)(2,1)S(1)}, u32[]{:S(2)}, u32[]{:S(2)}) async-start(bf16[16,256,128]{2,1,0:T(8,128)(2,1)} %bitcast.55), calls=%async_computation | async-start | bytes 2097152 | tf_op jit(solution)/shard_map/all_to_all | solution.py:22
  33.2 103.0 %copy-start.3 = (bf16[1,2048,264]{1,2,0:T(8,128)(2,1)S(1)}, bf16[1,2048,264]{1,2,0:T(8,128)(2,1)}, u32[]{:S(2)}) copy-start(bf16[1,2048,264]{1,2,0:T(8,128)(2,1)} %param.23) | copy-start | bytes 3244036
  56.3 9.7 %all-to-all-start.1 = ((f32[16,256,1]{1,2,0:T(1,128)}), f32[16,256,1]{1,2,0:T(1,128)S(1)}, u32[]{:S(2)}, u32[]{:S(2)}) async-start(f32[16,256,1]{1,2,0:T(1,128)} %broadcast_in_dim.67), calls=%async_computation.1 | async-start | bytes 32768 | tf_op jit(solution)/shard_map/all_to_all | solution.py:28
  61.5 74.6 %all-gather.2.cloned.1.call-start = ((), (), s32[]{:S(2)}) async-start(), calls=%async_computation.5 | async-start | bytes 3342336 | tf_op jit(solution)/shard_map/all_gather | solution.py:105
  94.2 45.8 %copy-start.4 = (bf16[1,2048,264]{1,2,0:T(8,128)(2,1)S(1)}, bf16[1,2048,264]{1,2,0:T(8,128)(2,1)}, u32[]{:S(2)}) copy-start(bf16[1,2048,264]{1,2,0:T(8,128)(2,1)} %param.24) | copy-start | bytes 3244036
  94.2 121.9 %reduce-scatter.4.cloned.1.call-start = ((), (), s32[]{:S(2)}) async-start(), calls=%async_computation.6 | async-start | bytes 3342336
  151.9 76.5 %copy-start.2 = (f32[256,2]{0,1:T(2,128)S(1)}, f32[256,2]{0,1:T(2,128)}, u32[]{:S(2)}) copy-start(f32[256,2]{0,1:T(2,128)} %param.22) | copy-start | bytes 6148
  217.9 20.2 %all-to-all-start.3 = ((bf16[32,24,128]{2,1,0:T(8,128)(2,1)}), bf16[32,24,128]{2,1,0:T(8,128)(2,1)S(1)}, u32[]{:S(2)}, u32[]{:S(2)}) async-start(bf16[32,24,128]{2,1,0:T(8,128)(2,1)} %bitcast.12), calls=%async_computation.3 | async-start | bytes 393216 | tf_op jit(solution)/shard_map/all_to_all | solution.py:111
Sparse Core Ops, SparseCore 0:
  94.3 41.7 all-gather.1
  152.1 63.9 reduce-scatter.3
where the time goes:
time: 250 us; the launch traced here: 249 us
  waiting for transfers between devices  138 us (55%)
  starting transfers between devices  30.3 us (12%)
  blocking collectives  25 us (10%)
  local copies, waits for them, and re-layouts  18.9 us (8%)
  between operations  13.7 us (5%)
  matrix products  12.7 us (5%)
  other arithmetic  10.6 us (4%)
    unnamed x3, waiting for transfers between devices  64.2 us
    all_gather x1, waiting for transfers between devices, shards(): piece_cols = lax.all_gather(row_block, 'tp', axis=1, tiled=True)  41.9 us
    all_to_all x1, blocking collectives, shards(): lax.all_to_all(picked, 'sp', split_axis=0, concat_axis=0, tiled=True)  25 us
    all_to_all x1, waiting for transfers between devices, sum_at_owner(): parts = lax.all_to_all(in_blocks(x, dim, count), axis, 0, 0, tiled=True)  21.4 us
    all_to_all x1, starting transfers between devices, shards(): lax.all_to_all(summed.reshape(experts, slot_count, share_width), 'sp', sp...  10.1 us
    all_to_all x1, waiting for transfers between devices, shards(): lax.all_to_all(summed.reshape(experts, slot_count, share_width), 'sp', sp...  9.51 us
    all_to_all x1, starting transfers between devices, sum_at_owner(): parts = lax.all_to_all(in_blocks(x, dim, count), axis, 0, 0, tiled=True)  8.75 us
    dot_general x1, matrix products, shards(): down_sum = jnp.dot(hidden, down_weight, preferred_element_type=jnp.float32)  7.29 us
  transfers between devices with their start and end apart: 7, of which 5 were waited for; matrix products, arithmetic and copies ran while one was open for 5% of the time, Pallas kernels for 0%

commit v1 on v0

--- a/solution.py
+++ b/solution.py
@@ -102,7 +102,9 @@
     arrived = lax.all_to_all(picked, "sp", split_axis=0, concat_axis=0, tiled=True)
     slot_count = arrived.shape[1]
     row_block = arrived.reshape(-1, share_width)
-    piece_cols = lax.all_gather(row_block, "tp", axis=1, tiled=True)
+    piece_cols = jnp.concatenate(
+        lax.all_to_all(jnp.stack([row_block] * lax.axis_size("tp")), "tp", 0, 0), axis=1
+    )
     gate_sum = jnp.dot(piece_cols, gate_weight, preferred_element_type=jnp.float32)
     up_sum = jnp.dot(piece_cols, up_weight, preferred_element_type=jnp.float32)
     hidden = (jax.nn.silu(gate_sum) * up_sum).astype(jnp.bfloat16)

time: 250 us -> 279 us (1.12)
  blocking collectives: 25 us -> 104 us
  waiting for transfers between devices: 138 us -> 89.1 us
  matrix products: 12.7 us -> 9.51 us
    all_to_all x0 -> x1, blocking collectives: none -> 78.8 us  [shards(): lax.all_to_all(jnp.stack([row_block] * lax.axis_size('tp')), 'tp', 0, 0)]
    all_gather x1 -> x0, waiting for transfers between devices: 41.9 us -> none  [shards(): piece_cols = lax.all_gather(row_block, 'tp', axis=1, tiled=True)]
    unnamed x3 -> x2, waiting for transfers between devices: 64.2 us -> 57.1 us
    dot_general x1, matrix products: 3.84 us -> 1.04 us  [shards(): jnp.dot(piece_cols, gate_weight, preferred_element_type=jnp.float32)]
    unnamed x14 -> x16, local copies, waits for them, and re-layouts: 6.67 us -> 8.59 us
  transfers between devices with their start and end apart: 7 -> 6, of which waited for: 5 -> 4; matrix products, arithmetic and copies ran while one was open for 5% -> 4% of each run, Pallas kernels for 0% -> 0%
where the time goes in v1:
time: 279 us; the launch traced here: 278 us
  blocking collectives  104 us (37%)
  waiting for transfers between devices  89.1 us (32%)
  starting transfers between devices  30.1 us (11%)
  local copies, waits for them, and re-layouts  21.2 us (8%)
  between operations  13.7 us (5%)
  other arithmetic  10.6 us (4%)
  matrix products  9.51 us (3%)
    all_to_all x1, blocking collectives, shards(): lax.all_to_all(jnp.stack([row_block] * lax.axis_size('tp')), 'tp', 0, 0)  78.8 us
    unnamed x2, waiting for transfers between devices  57.1 us
    all_to_all x1, blocking collectives, shards(): lax.all_to_all(picked, 'sp', split_axis=0, concat_axis=0, tiled=True)  24.9 us
    all_to_all x1, waiting for transfers between devices, sum_at_owner(): parts = lax.all_to_all(in_blocks(x, dim, count), axis, 0, 0, tiled=True)  21.4 us
    all_to_all x1, starting transfers between devices, shards(): lax.all_to_all(summed.reshape(experts, slot_count, share_width), 'sp', sp...  9.9 us
    all_to_all x1, waiting for transfers between devices, shards(): lax.all_to_all(summed.reshape(experts, slot_count, share_width), 'sp', sp...  9.55 us
    all_to_all x1, starting transfers between devices, sum_at_owner(): parts = lax.all_to_all(in_blocks(x, dim, count), axis, 0, 0, tiled=True)  8.75 us
    unnamed x16, local copies, waits for them, and re-layouts  8.59 us
  transfers between devices with their start and end apart: 6, of which 4 were waited for; matrix products, arithmetic and copies ran while one was open for 4% of the time, Pallas kernels for 0%

profile of v1, /device:TPU:25, one launch (start us, length us, event | category | flops | bytes accessed | tf_op | source)
XLA Modules:
  0.0 277.9 jit_solution(16135917556823916261)
XLA Ops:
  6.5 0.9 multiply_convert_fusion.1
  7.5 3.1 %collective-permute-start = (bf16[64,2]{1,0:T(8,128)(2,1)S(1)}, bf16[64,2]{1,0:T(8,128)(2,1)S(1)}, u32[]{:S(2)}, u32[]{:S(2)}) collective-permute-start(bf16[64,2]{1,0:T(8,128)(2,1)S(1)} %slice.52), channel_id=1, source_target_pairs={{0,16},{16,32},{32,48},{48,64},{64,80},{80,96},{96,112},{112,128},... | collective-permute-start | bytes 776 | tf_op jit(solution)/shard_map/ppermute | solution.py:12
  10.6 0.8 slice.41
  11.4 3.1 %collective-permute-start.1 = (s32[2]{0:T(128)S(1)}, s32[2]{0:T(128)S(1)}, u32[]{:S(2)}, u32[]{:S(2)}) collective-permute-start(s32[2]{0:T(128)S(1)} %slice.41), channel_id=1, source_target_pairs={{0,16},{16,32},{32,48},{48,64},{64,80},{80,96},{96,112},{112,128},... | collective-permute-start | bytes 32 | tf_op jit(solution)/shard_map/ppermute | solution.py:12
  15.2 0.8 pad_add_fusion
  15.9 0.8 compare_convert_fusion.1
  16.8 1.5 fusion
  18.3 1.3 copy.44
  19.6 8.7 %all-to-all-start = ((bf16[16,256,128]{2,1,0:T(8,128)(2,1)}), bf16[16,256,128]{2,1,0:T(8,128)(2,1)S(1)}, u32[]{:S(2)}, u32[]{:S(2)}) async-start(bf16[16,256,128]{2,1,0:T(8,128)(2,1)} %bitcast.58), calls=%async_computation | async-start | bytes 2097152 | tf_op jit(solution)/shard_map/all_to_all | solution.py:22
  28.8 1.2 reduce-window.6
  30.7 2.4 scatter_custom_fusion.1
  33.2 21.4 %all-to-all-done = bf16[16,256,128]{2,1,0:T(8,128)(2,1)S(1)} async-done(((bf16[16,256,128]{2,1,0:T(8,128)(2,1)}), bf16[16,256,128]{2,1,0:T(8,128)(2,1)S(1)}, u32[]{:S(2)}, u32[]{:S(2)}) %all-to-all-start) | async-done | bytes 1048608 | tf_op jit(solution)/shard_map/all_to_all | solution.py:22
  54.7 1.0 multiply_reduce_fusion.1
  56.3 5.2 %all-to-all-start.1 = ((f32[16,256,1]{1,2,0:T(1,128)}), f32[16,256,1]{1,2,0:T(1,128)S(1)}, u32[]{:S(2)}, u32[]{:S(2)}) async-start(f32[16,256,1]{1,2,0:T(1,128)} %broadcast_in_dim.67), calls=%async_computation.1 | async-start | bytes 32768 | tf_op jit(solution)/shard_map/all_to_all | solution.py:28
  61.5 0.8 dynamic-slice_convert_fusion
  62.4 2.4 scatter_custom_fusion
  65.0 1.1 all-to-all-done.1
  66.1 0.9 multiply_convert_fusion
  67.0 1.9 gather_fusion
  69.2 24.9 %all_to_all.25 = bf16[32,24,128]{2,1,0:T(8,128)(2,1)S(1)} all-to-all(bf16[32,24,128]{2,1,0:T(8,128)(2,1)S(1)} %select_select_fusion), channel_id=1, replica_groups=mesh['sp'=32,'tp'=16] {'sp'}, dimensions={0} | all-to-all | bytes 393216 | tf_op jit(solution)/shard_map/all_to_all | solution.py:102
  94.5 78.8 %all_to_all.26 = bf16[16,768,128]{1,2,0:T(8,128)(2,1)S(1)} all-to-all(bf16[16,768,128]{1,2,0:T(8,128)(2,1)S(1)} %stack.3), channel_id=1, replica_groups=mesh['sp'=32,'tp'=16] {'tp'}, dimensions={0} | all-to-all | bytes 6291456 | tf_op jit(solution)/shard_map/all_to_all | solution.py:106
  173.3 1.7 copy-done.1
  175.0 1.0 fusion.4
  176.3 6.9 %convolution_convert_fusion = bf16[768,2048]{1,0:T(8,128)(2,1)} fusion(bf16[1,264,2048]{2,1,0:T(8,128)(2,1)S(1)} %copy-done, bf16[768,2048]{0,1:T(8,128)(2,1)} %bitcast.62, bf16[1,2048,264]{1,2,0:T(8,128)(2,1)S(1)} %copy-done.5, f32[768,264]{0,1:T(8,128)S(1)} %fusion.4), kind=kOutput, calls=%fused_computation.4 | convolution fusion | flops 1663733760 | bytes 9265152 | tf_op jit(solution)/shard_map/dot_general | solution.py:111
  183.2 4.7 %copy.38 = bf16[768,2048]{0,1:T(8,128)(2,1)} copy(bf16[768,2048]{1,0:T(8,128)(2,1)} %convolution_convert_fusion) | data formatting | bytes 6291456
  187.9 57.1 %reduce-scatter.4.cloned.1.call-done = bf16[128,768]{1,0:T(8,128)(2,1)} async-done(((bf16[2048,768]{1,0:T(8,128)(2,1)}), bf16[128,768]{1,0:T(8,128)(2,1)}) %reduce-scatter.4.cloned.1.call-update) | async-done | bytes 196624
  245.0 1.7 copy.39
  246.7 9.9 %all-to-all-start.4 = ((bf16[32,24,128]{2,1,0:T(8,128)(2,1)}), bf16[32,24,128]{2,1,0:T(8,128)(2,1)S(1)}, u32[]{:S(2)}, u32[]{:S(2)}) async-start(bf16[32,24,128]{2,1,0:T(8,128)(2,1)} %bitcast.15), calls=%async_computation.4 | async-start | bytes 393216 | tf_op jit(solution)/shard_map/all_to_all | solution.py:113
  257.2 9.5 %all-to-all-done.4 = bf16[32,24,128]{2,1,0:T(8,128)(2,1)S(1)} async-done(((bf16[32,24,128]{2,1,0:T(8,128)(2,1)}), bf16[32,24,128]{2,1,0:T(8,128)(2,1)S(1)}, u32[]{:S(2)}, u32[]{:S(2)}) %all-to-all-start.4) | async-done | bytes 196640 | tf_op jit(solution)/shard_map/all_to_all | solution.py:113
  266.8 1.3 gather_fusion.1
  268.1 1.5 multiply_reduce_fusion
  269.6 1.5 add_convert_fusion
  (52 shorter events, 4.5 us)
Async XLA Ops:
  6.5 169.6 %copy-start = (bf16[1,264,2048]{2,1,0:T(8,128)(2,1)S(1)}, bf16[1,264,2048]{2,1,0:T(8,128)(2,1)}, u32[]{:S(2)}) copy-start(bf16[1,264,2048]{2,1,0:T(8,128)(2,1)} %param.25) | copy-start | bytes 3244036
  7.5 9.2 %collective-permute-start = (bf16[64,2]{1,0:T(8,128)(2,1)S(1)}, bf16[64,2]{1,0:T(8,128)(2,1)S(1)}, u32[]{:S(2)}, u32[]{:S(2)}) collective-permute-start(bf16[64,2]{1,0:T(8,128)(2,1)S(1)} %slice.52), channel_id=1, source_target_pairs={{0,16},{16,32},{32,48},{48,64},{64,80},{80,96},{96,112},{112,128},... | collective-permute-start | bytes 776 | tf_op jit(solution)/shard_map/ppermute | solution.py:12
  11.4 3.8 %collective-permute-start.1 = (s32[2]{0:T(128)S(1)}, s32[2]{0:T(128)S(1)}, u32[]{:S(2)}, u32[]{:S(2)}) collective-permute-start(s32[2]{0:T(128)S(1)} %slice.41), channel_id=1, source_target_pairs={{0,16},{16,32},{32,48},{48,64},{64,80},{80,96},{96,112},{112,128},... | collective-permute-start | bytes 32 | tf_op jit(solution)/shard_map/ppermute | solution.py:12
  18.3 10.0 %copy-start.2 = (s32[256,2]{0,1:T(2,128)S(1)}, s32[256,2]{0,1:T(2,128)}, u32[]{:S(2)}) copy-start(s32[256,2]{0,1:T(2,128)} %param.21) | copy-start | bytes 6148
  19.6 35.0 %all-to-all-start = ((bf16[16,256,128]{2,1,0:T(8,128)(2,1)}), bf16[16,256,128]{2,1,0:T(8,128)(2,1)S(1)}, u32[]{:S(2)}, u32[]{:S(2)}) async-start(bf16[16,256,128]{2,1,0:T(8,128)(2,1)} %bitcast.58), calls=%async_computation | async-start | bytes 2097152 | tf_op jit(solution)/shard_map/all_to_all | solution.py:22
  56.3 9.7 %all-to-all-start.1 = ((f32[16,256,1]{1,2,0:T(1,128)}), f32[16,256,1]{1,2,0:T(1,128)S(1)}, u32[]{:S(2)}, u32[]{:S(2)}) async-start(f32[16,256,1]{1,2,0:T(1,128)} %broadcast_in_dim.67), calls=%async_computation.1 | async-start | bytes 32768 | tf_op jit(solution)/shard_map/all_to_all | solution.py:28
  61.5 183.5 %reduce-scatter.4.cloned.1.call-start = ((), (), s32[]{:S(2)}) async-start(), calls=%async_computation.6 | async-start | bytes 3342336
  94.5 80.5 %copy-start.4 = (bf16[1,2048,264]{1,2,0:T(8,128)(2,1)S(1)}, bf16[1,2048,264]{1,2,0:T(8,128)(2,1)}, u32[]{:S(2)}) copy-start(bf16[1,2048,264]{1,2,0:T(8,128)(2,1)} %param.23) | copy-start | bytes 3244036
  173.3 1.7 copy-start.1
  175.0 1.2 copy-start.5
  187.9 69.2 %copy-start.3 = (f32[256,2]{0,1:T(2,128)S(1)}, f32[256,2]{0,1:T(2,128)}, u32[]{:S(2)}) copy-start(f32[256,2]{0,1:T(2,128)} %param.22) | copy-start | bytes 6148
  246.7 20.0 %all-to-all-start.4 = ((bf16[32,24,128]{2,1,0:T(8,128)(2,1)}), bf16[32,24,128]{2,1,0:T(8,128)(2,1)S(1)}, u32[]{:S(2)}, u32[]{:S(2)}) async-start(bf16[32,24,128]{2,1,0:T(8,128)(2,1)} %bitcast.15), calls=%async_computation.4 | async-start | bytes 393216 | tf_op jit(solution)/shard_map/all_to_all | solution.py:113
Sparse Core Ops, SparseCore 0:
  188.1 56.8 reduce-scatter.3
